TPU v7x, 32 devices: a whole 2x2x4 slice. The times are simulated.
32 devices in a mesh: kv: 4 (over y, x), tp: 8 (over z, core).
Axes of the slice: x: 2, y: 2, z: 4, core: 2. Of those that a mesh axis runs over, the one named last changes fastest.
Arguments:
- tokens: bfloat16 [256, 4096], P(None, ('kv', 'tp')), may hold values from -10 to 10
- past_state: float32 [256, 32, 64, 128], P('kv', 'tp'), may hold values from -6 to 6
- first_gain: float32 [4096], P('kv'), may hold values from 0.1 to 1.9
- first_gate: bfloat16 [4096, 11264], P('kv', 'tp'), may hold values from -0.09375 to 0.09375
- first_up: bfloat16 [4096, 11264], P('kv', 'tp'), may hold values from -0.09375 to 0.09375
- first_down: bfloat16 [11264, 4096], P('tp', 'kv'), may hold values from -0.078125 to 0.078125
- mix_gain: float32 [4096], P('kv'), may hold values from 0.1 to 1.9
- query_weight: bfloat16 [4096, 2048], P('kv', 'tp'), may hold values from -0.09375 to 0.09375
- key_weight: bfloat16 [4096, 2048], P('kv', 'tp'), may hold values from -0.09375 to 0.09375
- value_weight: bfloat16 [4096, 4096], P('kv', 'tp'), may hold values from -0.09375 to 0.09375
- output_gate_weight: bfloat16 [4096, 4096], P('kv', 'tp'), may hold values from -0.09375 to 0.09375
- head_gain: float32 [4096], P('tp'), may hold values from 0.1 to 1.9
- out_weight: bfloat16 [4096, 4096], P('tp', 'kv'), may hold values from -0.125 to 0.125
- second_gain: float32 [4096], P('kv'), may hold values from 0.1 to 1.9
- second_gate: bfloat16 [4096, 11264], P('kv', 'tp'), may hold values from -0.09375 to 0.09375
- second_up: bfloat16 [4096, 11264], P('kv', 'tp'), may hold values from -0.09375 to 0.09375
- second_down: bfloat16 [11264, 4096], P('tp', 'kv'), may hold values from -0.078125 to 0.078125
Outputs:
- mixed: bfloat16 [256, 4096], P(None, ('kv', 'tp'))
- new_state: float32 [256, 32, 64, 128], P('kv', 'tp')
All inputs are finite; a program needn't handle non-finite values.
Results may differ from a plain program's by a relative error of at most 0.033.
Values may be sent and summed in bfloat16 or wider, within the bound.
A program may use at most 128 MiB of HBM per device.

v0:
```python
import jax
import jax.numpy as jnp
from jax import lax
from jax.sharding import PartitionSpec as P

D = 4096
HEADS = 32
HEAD_K = 64
HEAD_V = 128
POS = 16384
EPS_RMS = 1e-06
EPS_GROUP = 1e-05
ROPE_BASE = 10000.0


def rotate(vectors):
    half_width = vectors.shape[-1] // 2
    frequency = ROPE_BASE ** (-jnp.arange(half_width, dtype=jnp.float32) / half_width)
    angles = POS * frequency
    cosine = jnp.cos(angles)
    sine_part = jnp.sin(angles)
    lower = vectors[..., :half_width]
    upper = vectors[..., half_width:]
    return jnp.concatenate(
        [lower * cosine - upper * sine_part, lower * sine_part + upper * cosine], axis=-1
    )


def activate(gate_sum, up_sum, summed):
    inverse_rms = lax.rsqrt(summed / D + EPS_RMS)[:, None]
    return (jax.nn.silu(gate_sum * inverse_rms) * (up_sum * inverse_rms)).astype(jnp.bfloat16)


def channel_mix(widened, gain, w_gate, w_up, w_down):
    widened_f = widened.astype(jnp.float32)
    scaled = (widened_f * gain).astype(jnp.bfloat16)
    squares = jnp.sum(widened_f * widened_f, axis=1)
    gate_part = jnp.dot(scaled, w_gate, preferred_element_type=jnp.float32)
    up_part = jnp.dot(scaled, w_up, preferred_element_type=jnp.float32)
    gate_sum, up_sum, summed = (
        lax.psum(gate_part.astype(jnp.bfloat16), "kv").astype(jnp.float32),
        lax.psum(up_part.astype(jnp.bfloat16), "kv").astype(jnp.float32),
        lax.psum(squares.astype(jnp.bfloat16), "kv").astype(jnp.float32),
    )
    return 0.5 * jnp.dot(
        activate(gate_sum, up_sum, summed), w_down, preferred_element_type=jnp.float32
    )


def token_mix(
    widened,
    past_state,
    gain,
    query_weight,
    key_weight,
    value_weight,
    output_gate_weight,
    head_gain,
    out_weight,
):
    widened_f = widened.astype(jnp.float32)
    scaled = (widened_f * gain).astype(jnp.bfloat16)
    squares = jnp.sum(widened_f * widened_f, axis=1)
    query_part = jnp.dot(scaled, query_weight, preferred_element_type=jnp.float32)
    key_part = jnp.dot(scaled, key_weight, preferred_element_type=jnp.float32)
    value_part = jnp.dot(scaled, value_weight, preferred_element_type=jnp.float32)
    gate_part = jnp.dot(scaled, output_gate_weight, preferred_element_type=jnp.float32)
    queries, keys_now, values_now, gate_now, summed = (
        lax.psum_scatter(
            query_part.astype(jnp.bfloat16), "kv", scatter_dimension=0, tiled=True
        ).astype(jnp.float32),
        lax.psum_scatter(
            key_part.astype(jnp.bfloat16), "kv", scatter_dimension=0, tiled=True
        ).astype(jnp.float32),
        lax.psum_scatter(
            value_part.astype(jnp.bfloat16), "kv", scatter_dimension=0, tiled=True
        ).astype(jnp.float32),
        lax.psum_scatter(
            gate_part.astype(jnp.bfloat16), "kv", scatter_dimension=0, tiled=True
        ).astype(jnp.float32),
        lax.psum_scatter(
            squares.astype(jnp.bfloat16), "kv", scatter_dimension=0, tiled=True
        ).astype(jnp.float32),
    )
    inverse_rms = lax.rsqrt(summed / D + EPS_RMS)[:, None]
    row_count = past_state.shape[0]
    local_heads = past_state.shape[1]
    queries = rotate((queries * inverse_rms).reshape(row_count, local_heads, HEAD_K)) * HEAD_K ** (
        -0.5
    )
    keys_now = rotate((keys_now * inverse_rms).reshape(row_count, local_heads, HEAD_K))
    values_now = (values_now * inverse_rms).reshape(row_count, local_heads, HEAD_V)
    gate_now = gate_now * inverse_rms
    head_level = (lax.axis_index("tp") * local_heads + jnp.arange(local_heads)).astype(jnp.float32)
    retained = 1.0 - jnp.exp2(-5.0 - 16.0 * head_level / (HEADS - 1))
    new_state = (
        retained[None, :, None, None] * past_state
        + keys_now[:, :, :, None] * values_now[:, :, None, :]
    )
    retrieved = jnp.einsum("bhk,bhkv->bhv", queries, new_state, precision=lax.Precision.HIGHEST)
    head_mean = jnp.mean(retrieved, axis=-1, keepdims=True)
    variance = jnp.mean(jnp.square(retrieved - head_mean), axis=-1, keepdims=True)
    normed = ((retrieved - head_mean) * lax.rsqrt(variance + EPS_GROUP)).reshape(
        row_count, local_heads * HEAD_V
    )
    mixed_heads = (jax.nn.silu(gate_now) * (normed * head_gain)).astype(jnp.bfloat16)
    projected = jnp.dot(
        lax.all_gather(mixed_heads, "kv", axis=0, tiled=True),
        out_weight,
        preferred_element_type=jnp.float32,
    )
    return (projected, new_state)


def shards(
    tokens,
    past_state,
    first_gain,
    first_gate,
    first_up,
    first_down,
    mix_gain,
    query_weight,
    key_weight,
    value_weight,
    output_gate_weight,
    head_gain,
    out_weight,
    second_gain,
    second_gate,
    second_up,
    second_down,
):

    def first_section(widened):
        return (channel_mix(widened, first_gain, first_gate, first_up, first_down), None)

    def middle_section(widened):
        return token_mix(
            widened,
            past_state,
            mix_gain,
            query_weight,
            key_weight,
            value_weight,
            output_gate_weight,
            head_gain,
            out_weight,
        )

    def last_section(widened):
        return (channel_mix(widened, second_gain, second_gate, second_up, second_down), None)

    sections = [first_section, middle_section, last_section]
    own_columns = tokens
    widened = lax.all_gather(tokens, "tp", axis=1, tiled=True)
    state_out = past_state
    for section_index in range(3):
        branch_out, produced = sections[section_index](widened)
        if produced is not None:
            state_out = produced
        own_piece = lax.psum_scatter(
            branch_out.astype(jnp.bfloat16), "tp", scatter_dimension=1, tiled=True
        ).astype(jnp.float32)
        own_columns = (own_columns.astype(jnp.float32) + own_piece).astype(jnp.bfloat16)
        if section_index < 2:
            widened = lax.all_gather(own_columns, "tp", axis=1, tiled=True)
    return (own_columns, state_out)


def solution(mesh):
    in_specs = (
        P(None, ("kv", "tp")),
        P("kv", "tp", None, None),
        P("kv"),
        P("kv", "tp"),
        P("kv", "tp"),
        P("tp", "kv"),
        P("kv"),
        P("kv", "tp"),
        P("kv", "tp"),
        P("kv", "tp"),
        P("kv", "tp"),
        P("tp"),
        P("tp", "kv"),
        P("kv"),
        P("kv", "tp"),
        P("kv", "tp"),
        P("tp", "kv"),
    )
    out_specs = (P(None, ("kv", "tp")), P("kv", "tp", None, None))
    return jax.shard_map(shards, mesh=mesh, in_specs=in_specs, out_specs=out_specs, check_vma=False)
```

profile of v0, /device:TPU:0, one launch (start us, length us, event | category | flops | bytes accessed | tf_op | source)
XLA Modules:
  0.0 409.7 jit_solution(10858656113238108868)
XLA Ops:
  7.2 15.8 %all_gather.12 = bf16[256,1024]{1,0:T(8,128)(2,1)S(1)} all-gather(bf16[256,128]{1,0:T(8,128)(2,1)} %param.17), channel_id=1, replica_groups=mesh['kv'=4,'tp'=8] {'tp'}, dimensions={1}, use_global_device_ids=true | all-gather | bytes 589824 | tf_op jit(solution)/shard_map/all_gather | solution.py:156
  23.0 2.5 convolution_convert_fusion.2
  25.6 1.9 convolution_convert_fusion.3
  27.5 0.2 fusion.3
  27.7 10.1 %psum.43 = bf16[256]{0:T(256)(128)(2,1)S(1)} all-reduce(bf16[256]{0:T(256)(128)(2,1)S(1)} %fusion.3), channel_id=1, replica_groups=mesh['kv'=4,'tp'=8] {'kv'}, use_global_device_ids=true, to_apply=%region_2.0 | all-reduce | flops 256 | bytes 1024 | tf_op jit(solution)/shard_map/psum | solution.py:43
  37.8 48.4 %all-reduce.8.cloned.1.call-done = (bf16[256,1408]{1,0:T(8,128)(2,1)}, bf16[256,1408]{1,0:T(8,128)(2,1)}) async-done(((bf16[256,1408]{1,0:T(8,128)(2,1)}, bf16[256,1408]{1,0:T(8,128)(2,1)}), (bf16[256,1408]{1,0:T(8,128)(2,1)}, bf16[256,1408]{1,0:T(8,128)(2,1)})) %all-reduce.8.cloned.1.call-update) | async-done | bytes 1441808 | tf_op jit(solution)/shard_map/psum | solution.py:42
  86.2 3.5 fusion
  89.7 1.0 copy.24
  90.8 31.2 %reduce-scatter.22.cloned.1.call-done = bf16[128,256]{1,0:T(8,128)(2,1)} async-done(((bf16[1024,256]{1,0:T(8,128)(2,1)}), bf16[128,256]{1,0:T(8,128)(2,1)}) %reduce-scatter.22.cloned.1.call-update) | async-done | bytes 65552
  122.0 0.9 copy.25
  123.0 14.0 %all_gather.13 = bf16[256,1024]{1,0:T(8,128)(2,1)S(1)} all-gather(bf16[256,128]{1,0:T(8,128)(2,1)S(1)} %add_convert_fusion.2), channel_id=1, replica_groups=mesh['kv'=4,'tp'=8] {'tp'}, dimensions={1}, use_global_device_ids=true | all-gather | bytes 589824 | tf_op jit(solution)/shard_map/all_gather | solution.py:167
  137.1 2.0 convolution_convert_fusion.8
  139.2 0.6 dynamic-slice
  140.4 2.0 convolution_convert_fusion.7
  142.5 2.4 convolution_convert_fusion.5
  144.9 0.2 fusion.5
  145.1 9.9 %all-reduce = bf16[256]{0:T(256)(128)(2,1)S(1)} all-reduce(bf16[256]{0:T(256)(128)(2,1)S(1)} %fusion.5), channel_id=4, replica_groups=mesh['kv'=4,'tp'=8] {'kv'}, use_global_device_ids=true, to_apply=%region_7.8.clone | all-reduce | flops 256 | bytes 1024
  155.2 2.4 convolution_convert_fusion.6
  157.6 0.2 reduce-scatter.24.cloned.1.call-start
  157.8 4.2 %reduce-scatter.16.cloned.1.call-done = bf16[64,256]{1,0:T(8,128)(2,1)} async-done(((bf16[256,256]{1,0:T(8,128)(2,1)}), bf16[64,256]{1,0:T(8,128)(2,1)}) %reduce-scatter.16.cloned.1.call-update) | async-done | bytes 32784 | tf_op jit(solution)/shard_map/reduce_scatter | solution.py:69
  162.0 26.8 %reduce-scatter.18.cloned.1.call-done = bf16[64,256]{1,0:T(8,128)(2,1)} async-done(((bf16[256,256]{1,0:T(8,128)(2,1)}), bf16[64,256]{1,0:T(8,128)(2,1)}) %reduce-scatter.18.cloned.1.call-update) | async-done | bytes 32784 | tf_op jit(solution)/shard_map/reduce_scatter | solution.py:72
  188.8 0.8 convert_multiply_fusion.7
  190.0 0.1 copy.21
  190.2 26.1 %reduce-scatter.20.cloned.1.call-done = bf16[64,512]{1,0:T(8,128)(2,1)} async-done(((bf16[256,512]{1,0:T(8,128)(2,1)}), bf16[64,512]{1,0:T(8,128)(2,1)}) %reduce-scatter.20.cloned.1.call-update) | async-done | bytes 65552 | tf_op jit(solution)/shard_map/reduce_scatter | solution.py:75
  216.3 0.9 convert_multiply_fusion.6
  217.3 5.3 %multiply_add_fusion = f32[64,4,64,128]{3,2,1,0:T(8,128)S(1)} fusion(f32[64,4,64,128]{3,2,1,0:T(8,128)} %param.18, f32[64,4,128]{2,1,0:T(4,128)S(1)} %mul.290, f32[64,4,64]{2,1,0:T(4,128)S(1)} %copy.21, f32[4]{0:T(128)S(1)} %exponential_subtract_fusion), kind=kLoop, calls=%fused_computation | loop fusion | flops 6291456 | bytes 16973840 | tf_op jit(solution)/shard_map/add | solution.py:97
  222.6 7.3 %fusion.30 = f32[64,4,1,128]{3,2,1,0:T(1,128)S(1)} fusion(f32[64,4,64,1]{2,3,1,0:T(1,128)S(1)} %copy.22, f32[64,4,64,128]{3,2,1,0:T(8,128)S(1)} %multiply_add_fusion), kind=kOutput, calls=%fused_computation.64 | convolution fusion | flops 25165824 | bytes 8585216 | tf_op jit(solution)/shard_map/bhk,bhkv->bhv/dot_general | solution.py:100
  230.0 0.1 reduce_sum.47
  230.1 0.2 multiply_reduce_fusion
  230.4 0.2 subtract_multiply_fusion
  230.6 12.7 %reduce-scatter.14.cloned.1.call-done = bf16[64,512]{1,0:T(8,128)(2,1)} async-done(((bf16[256,512]{1,0:T(8,128)(2,1)}), bf16[64,512]{1,0:T(8,128)(2,1)}) %reduce-scatter.14.cloned.1.call-update) | async-done | bytes 65552 | tf_op jit(solution)/shard_map/reduce_scatter | solution.py:78
  243.3 1.0 fusion.21
  244.3 9.3 %all_gather.14 = bf16[256,512]{1,0:T(8,128)(2,1)S(1)} all-gather(bf16[64,512]{1,0:T(8,128)(2,1)S(1)} %fusion.21), channel_id=1, replica_groups=mesh['kv'=4,'tp'=8] {'kv'}, dimensions={0}, use_global_device_ids=true | all-gather | bytes 327680 | tf_op jit(solution)/shard_map/all_gather | solution.py:108
  253.6 1.7 convolution_convert_fusion.4
  255.2 1.0 copy.26
  256.3 31.4 %reduce-scatter.24.cloned.1.call-done = bf16[128,256]{1,0:T(8,128)(2,1)} async-done(((bf16[1024,256]{1,0:T(8,128)(2,1)}), bf16[128,256]{1,0:T(8,128)(2,1)}) %reduce-scatter.24.cloned.1.call-update) | async-done | bytes 65552
  287.7 0.9 copy.27
  288.7 14.2 %all_gather.15 = bf16[256,1024]{1,0:T(8,128)(2,1)S(1)} all-gather(bf16[256,128]{1,0:T(8,128)(2,1)S(1)} %add_convert_fusion.1), channel_id=1, replica_groups=mesh['kv'=4,'tp'=8] {'tp'}, dimensions={1}, use_global_device_ids=true | all-gather | bytes 589824 | tf_op jit(solution)/shard_map/all_gather | solution.py:167
  302.8 3.7 convolution_convert_fusion
  306.5 1.9 convolution_convert_fusion.1
  308.5 0.2 fusion.7
  308.6 10.2 %psum.46 = bf16[256]{0:T(256)(128)(2,1)S(1)} all-reduce(bf16[256]{0:T(256)(128)(2,1)S(1)} %fusion.7), channel_id=1, replica_groups=mesh['kv'=4,'tp'=8] {'kv'}, use_global_device_ids=true, to_apply=%region_16.17 | all-reduce | flops 256 | bytes 1024 | tf_op jit(solution)/shard_map/psum | solution.py:43
  318.9 46.7 %all-reduce.6.cloned.1.call-done = (bf16[256,1408]{1,0:T(8,128)(2,1)}, bf16[256,1408]{1,0:T(8,128)(2,1)}) async-done(((bf16[256,1408]{1,0:T(8,128)(2,1)}, bf16[256,1408]{1,0:T(8,128)(2,1)}), (bf16[256,1408]{1,0:T(8,128)(2,1)}, bf16[256,1408]{1,0:T(8,128)(2,1)})) %all-reduce.6.cloned.1.call-update) | async-done | bytes 1441808 | tf_op jit(solution)/shard_map/psum | solution.py:42
  365.6 3.4 fusion.1
  369.0 1.0 copy.28
  370.0 31.6 %reduce-scatter.26.cloned.1.call-done = bf16[128,256]{1,0:T(8,128)(2,1)} async-done(((bf16[1024,256]{1,0:T(8,128)(2,1)}), bf16[128,256]{1,0:T(8,128)(2,1)}) %reduce-scatter.26.cloned.1.call-update) | async-done | bytes 65552
  401.6 0.9 copy.29
  402.5 0.7 add_convert_fusion
  (53 shorter events, 1.2 us)
Async XLA Ops:
  7.2 15.9 %copy-start = (bf16[1024,1408]{1,0:T(8,128)(2,1)S(1)}, bf16[1024,1408]{1,0:T(8,128)(2,1)}, u32[]{:S(2)}) copy-start(bf16[1024,1408]{1,0:T(8,128)(2,1)} %param.21) | copy-start | bytes 8650756
  7.2 18.4 %copy-start.6 = (f32[1024]{0:T(1024)S(1)}, f32[1024]{0:T(1024)}, u32[]{:S(2)}) copy-start(f32[1024]{0:T(1024)} %param.19) | copy-start | bytes 12292
  7.2 79.0 %all-reduce.8.cloned.1.call-start = ((), (), s32[]{:S(2)}) async-start(), calls=%async_computation.15 | async-start | bytes 2883584 | tf_op jit(solution)/shard_map/psum | solution.py:42
  7.2 18.3 %copy-start.4 = (bf16[1024,1408]{1,0:T(8,128)(2,1)S(1)}, bf16[1024,1408]{1,0:T(8,128)(2,1)}, u32[]{:S(2)}) copy-start(bf16[1024,1408]{1,0:T(8,128)(2,1)} %param.20) | copy-start | bytes 8650756
  27.5 94.6 %reduce-scatter.22.cloned.1.call-start = ((), (), s32[]{:S(2)}) async-start(), calls=%async_computation.11 | async-start | bytes 589824
  86.2 36.8 %copy-start.2 = (bf16[256,128]{1,0:T(8,128)(2,1)S(1)}, bf16[256,128]{1,0:T(8,128)(2,1)}, u32[]{:S(2)}) copy-start(bf16[256,128]{1,0:T(8,128)(2,1)} %param.17) | copy-start | bytes 196612
  86.2 50.9 %copy-start.7 = (f32[1024]{0:T(1024)S(1)}, f32[1024]{0:T(1024)}, u32[]{:S(2)}) copy-start(f32[1024]{0:T(1024)} %param.23) | copy-start | bytes 12292
  89.7 49.5 %copy-start.9 = (u32[32]{0:T(128)S(1)}, u32[32]{0:T(128)}, u32[]{:S(2)}) copy-start(u32[32]{0:T(128)} %constant.53) | copy-start | bytes 388
  90.7 71.3 %reduce-scatter.16.cloned.1.call-start = ((), (), s32[]{:S(2)}) async-start(), calls=%async_computation.8 | async-start | bytes 163840 | tf_op jit(solution)/shard_map/reduce_scatter | solution.py:69
  139.1 49.7 %reduce-scatter.18.cloned.1.call-start = ((), (), s32[]{:S(2)}) async-start(), calls=%async_computation.9 | async-start | bytes 163840 | tf_op jit(solution)/shard_map/reduce_scatter | solution.py:72
  142.4 73.9 %reduce-scatter.20.cloned.1.call-start = ((), (), s32[]{:S(2)}) async-start(), calls=%async_computation.10 | async-start | bytes 327680 | tf_op jit(solution)/shard_map/reduce_scatter | solution.py:75
  144.9 98.4 %reduce-scatter.14.cloned.1.call-start = ((), (), s32[]{:S(2)}) async-start(), calls=%async_computation.7 | async-start | bytes 327680 | tf_op jit(solution)/shard_map/reduce_scatter | solution.py:78
  157.6 130.1 %reduce-scatter.24.cloned.1.call-start = ((), (), s32[]{:S(2)}) async-start(), calls=%async_computation.12 | async-start | bytes 589824
  222.6 7.4 %copy-start.1 = (f32[64,4,64,128]{3,2,1,0:T(8,128)}, f32[64,4,64,128]{3,2,1,0:T(8,128)S(1)}, u32[]{:S(2)}) copy-start(f32[64,4,64,128]{3,2,1,0:T(8,128)S(1)} %multiply_add_fusion) | copy-start | bytes 25165828
  222.6 20.7 %copy-start.3 = (f32[512]{0:T(512)S(1)}, f32[512]{0:T(512)}, u32[]{:S(2)}) copy-start(f32[512]{0:T(512)} %param.28) | copy-start | bytes 6148
  230.0 72.8 %copy-start.8 = (f32[1024]{0:T(1024)S(1)}, f32[1024]{0:T(1024)}, u32[]{:S(2)}) copy-start(f32[1024]{0:T(1024)} %param.30) | copy-start | bytes 12292
  256.2 109.3 %all-reduce.6.cloned.1.call-start = ((), (), s32[]{:S(2)}) async-start(), calls=%async_computation.14 | async-start | bytes 2883584 | tf_op jit(solution)/shard_map/psum | solution.py:42
  288.6 17.9 %copy-start.5 = (bf16[1024,1408]{1,0:T(8,128)(2,1)S(1)}, bf16[1024,1408]{1,0:T(8,128)(2,1)}, u32[]{:S(2)}) copy-start(bf16[1024,1408]{1,0:T(8,128)(2,1)} %param.31) | copy-start | bytes 8650756
  308.4 93.2 %reduce-scatter.26.cloned.1.call-start = ((), (), s32[]{:S(2)}) async-start(), calls=%async_computation.13 | async-start | bytes 589824
Sparse Core Ops, SparseCore 0:
  27.6 58.5 all-reduce.7
  90.8 31.1 reduce-scatter.21
  139.2 22.7 reduce-scatter.15
  164.6 24.1 reduce-scatter.17
  192.0 24.3 reduce-scatter.19
  218.9 24.3 reduce-scatter.13
  256.4 31.2 reduce-scatter.23
  308.5 56.9 all-reduce.5
  370.1 31.3 reduce-scatter.25
where the time goes:
time: 411 us; the launch traced here: 410 us
  waiting for transfers between devices  259 us (63%)
  blocking collectives  83.5 us (20%)
  matrix products  34.6 us (8%)
  between operations  14.8 us (4%)
  other arithmetic  10.2 us (2%)
  local copies, waits for them, and re-layouts  6.92 us (2%)
    psum x2, waiting for transfers between devices, channel_mix(): lax.psum(up_part.astype(jnp.bfloat16), 'kv').astype(jnp.float32)  95.1 us
    unnamed x12, waiting for transfers between devices  94.3 us
    all_gather x2, blocking collectives, shards(): widened = lax.all_gather(own_columns, 'tp', axis=1, tiled=True)  28.2 us
    reduce_scatter x1, waiting for transfers between devices, token_mix(): lax.psum_scatter(key_part.astype(jnp.bfloat16), 'kv', scatter_dimension=0...  26.8 us
    reduce_scatter x1, waiting for transfers between devices, token_mix(): lax.psum_scatter(value_part.astype(jnp.bfloat16), 'kv', scatter_dimension...  26.1 us
    psum x2, blocking collectives, channel_mix(): lax.psum(squares.astype(jnp.bfloat16), 'kv').astype(jnp.float32)  20.3 us
    all_gather x1, blocking collectives, shards(): widened = lax.all_gather(tokens, 'tp', axis=1, tiled=True)  15.8 us
    reduce_scatter x1, waiting for transfers between devices, token_mix(): lax.psum_scatter(gate_part.astype(jnp.bfloat16), 'kv', scatter_dimension=...  12.7 us
  transfers between devices with their start and end apart: 9, of which 9 were waited for; matrix products, arithmetic and copies ran while one was open for 6% of the time, Pallas kernels for 0%

commit v1 on v0

--- a/solution.py
+++ b/solution.py
@@ -2,6 +2,7 @@
 import jax.numpy as jnp
 from jax import lax
 from jax.sharding import PartitionSpec as P
+from jax.lax import all_gather
 
 D = 4096
 HEADS = 32
@@ -39,7 +40,9 @@
     up_part = jnp.dot(scaled, w_up, preferred_element_type=jnp.float32)
     gate_sum, up_sum, summed = (
         lax.psum(gate_part.astype(jnp.bfloat16), "kv").astype(jnp.float32),
-        lax.psum(up_part.astype(jnp.bfloat16), "kv").astype(jnp.float32),
+        jnp.sum(all_gather(up_part.astype(jnp.bfloat16), axis_name="kv"), axis=0).astype(
+            jnp.float32
+        ),
         lax.psum(squares.astype(jnp.bfloat16), "kv").astype(jnp.float32),
     )
     return 0.5 * jnp.dot(

time: 411 us -> 474 us (1.15)
  waiting for transfers between devices: 259 us -> 313 us
  other arithmetic: 10.2 us -> 16.7 us
    all_gather x0 -> x2, waiting for transfers between devices: none -> 53.5 us  [channel_mix(): all_gather(up_part.astype(jnp.bfloat16), axis_name='kv')]
    reduce_sum x0 -> x2, other arithmetic: none -> 6.58 us  [channel_mix(): jnp.sum(all_gather(up_part.astype(jnp.bfloat16), axis_name='kv'), axis=0)]
    unnamed x12 -> x14, waiting for transfers between devices: 94.3 us -> 94.6 us
  transfers between devices with their start and end apart: 9 -> 11, of which waited for: 9 -> 11; matrix products, arithmetic and copies ran while one was open for 6% -> 8% of each run, Pallas kernels for 0% -> 0%
where the time goes in v1:
time: 474 us; the launch traced here: 473 us
  waiting for transfers between devices  313 us (66%)
  blocking collectives  83.4 us (18%)
  matrix products  38.2 us (8%)
  other arithmetic  16.7 us (4%)
  between operations  14.8 us (3%)
  local copies, waits for them, and re-layouts  6.91 us (1%)
    psum x2, waiting for transfers between devices, channel_mix(): lax.psum(gate_part.astype(jnp.bfloat16), 'kv').astype(jnp.float32)  94.8 us
    unnamed x14, waiting for transfers between devices  94.6 us
    all_gather x2, waiting for transfers between devices, channel_mix(): all_gather(up_part.astype(jnp.bfloat16), axis_name='kv')  53.5 us
    all_gather x2, blocking collectives, shards(): widened = lax.all_gather(own_columns, 'tp', axis=1, tiled=True)  28 us
    reduce_scatter x1, waiting for transfers between devices, token_mix(): lax.psum_scatter(key_part.astype(jnp.bfloat16), 'kv', scatter_dimension=0...  26.8 us
    reduce_scatter x1, waiting for transfers between devices, token_mix(): lax.psum_scatter(value_part.astype(jnp.bfloat16), 'kv', scatter_dimension...  26.1 us
    psum x2, blocking collectives, channel_mix(): lax.psum(squares.astype(jnp.bfloat16), 'kv').astype(jnp.float32)  20.6 us
    all_gather x1, blocking collectives, shards(): widened = lax.all_gather(tokens, 'tp', axis=1, tiled=True)  15.8 us
  transfers between devices with their start and end apart: 11, of which 11 were waited for; matrix products, arithmetic and copies ran while one was open for 8% of the time, Pallas kernels for 0%

profile of v1, /device:TPU:0, one launch (start us, length us, event | category | flops | bytes accessed | tf_op | source)
XLA Modules:
  0.0 473.5 jit_solution(7350168983002603778)
XLA Ops:
  7.2 15.8 %all_gather.24 = bf16[256,1024]{1,0:T(8,128)(2,1)S(1)} all-gather(bf16[256,128]{1,0:T(8,128)(2,1)} %param.17), channel_id=1, replica_groups=mesh['kv'=4,'tp'=8] {'tp'}, dimensions={1}, use_global_device_ids=true | all-gather | bytes 589824 | tf_op jit(solution)/shard_map/all_gather | solution.py:159
  23.0 2.6 convolution_convert_fusion.2
  25.7 3.7 convolution_convert_fusion.3
  29.4 0.2 fusion.3
  29.6 10.2 %psum.29 = bf16[256]{0:T(256)(128)(2,1)S(1)} all-reduce(bf16[256]{0:T(256)(128)(2,1)S(1)} %fusion.3), channel_id=1, replica_groups=mesh['kv'=4,'tp'=8] {'kv'}, use_global_device_ids=true, to_apply=%region_2.0 | all-reduce | flops 256 | bytes 1024 | tf_op jit(solution)/shard_map/psum | solution.py:46
  39.9 27.5 %all-gather.5.cloned.1.call-done = bf16[1024,1408]{1,0:T(8,128)(2,1)} async-done(((bf16[256,1408]{1,0:T(8,128)(2,1)}), bf16[1024,1408]{1,0:T(8,128)(2,1)}) %all-gather.5.cloned.1.call-update) | async-done | bytes 2883600 | tf_op jit(solution)/shard_map/all_gather | solution.py:43
  67.4 3.3 reduce_sum.70
  70.7 47.5 %all-reduce.4.cloned.1.call-done = bf16[256,1408]{1,0:T(8,128)(2,1)} async-done(((bf16[256,1408]{1,0:T(8,128)(2,1)}), bf16[256,1408]{1,0:T(8,128)(2,1)}) %all-reduce.4.cloned.1.call-update) | async-done | bytes 720912 | tf_op jit(solution)/shard_map/psum | solution.py:42
  118.2 3.4 fusion
  121.6 1.0 copy.24
  122.8 31.5 %reduce-scatter.22.cloned.1.call-done = bf16[128,256]{1,0:T(8,128)(2,1)} async-done(((bf16[1024,256]{1,0:T(8,128)(2,1)}), bf16[128,256]{1,0:T(8,128)(2,1)}) %reduce-scatter.22.cloned.1.call-update) | async-done | bytes 65552
  154.2 0.9 copy.25
  155.2 14.0 %all_gather.27 = bf16[256,1024]{1,0:T(8,128)(2,1)S(1)} all-gather(bf16[256,128]{1,0:T(8,128)(2,1)S(1)} %add_convert_fusion.2), channel_id=1, replica_groups=mesh['kv'=4,'tp'=8] {'tp'}, dimensions={1}, use_global_device_ids=true | all-gather | bytes 589824 | tf_op jit(solution)/shard_map/all_gather | solution.py:170
  169.2 2.0 convolution_convert_fusion.8
  171.4 0.6 dynamic-slice
  172.6 2.0 convolution_convert_fusion.7
  174.7 2.4 convolution_convert_fusion.5
  177.3 9.7 %all-reduce = bf16[256]{0:T(256)(128)(2,1)S(1)} all-reduce(bf16[256]{0:T(256)(128)(2,1)S(1)} %fusion.5), channel_id=6, replica_groups=mesh['kv'=4,'tp'=8] {'kv'}, use_global_device_ids=true, to_apply=%region_7.8.clone | all-reduce | flops 256 | bytes 1024
  187.1 2.4 convolution_convert_fusion.6
  189.5 0.2 reduce-scatter.24.cloned.1.call-start
  189.7 4.2 reduce-scatter.16.cloned.1.call-done
  193.9 26.8 %reduce-scatter.18.cloned.1.call-done = bf16[64,256]{1,0:T(8,128)(2,1)} async-done(((bf16[256,256]{1,0:T(8,128)(2,1)}), bf16[64,256]{1,0:T(8,128)(2,1)}) %reduce-scatter.18.cloned.1.call-update) | async-done | bytes 32784 | tf_op jit(solution)/shard_map/reduce_scatter | solution.py:75
  220.7 0.8 convert_multiply_fusion.7
  222.1 26.1 %reduce-scatter.20.cloned.1.call-done = bf16[64,512]{1,0:T(8,128)(2,1)} async-done(((bf16[256,512]{1,0:T(8,128)(2,1)}), bf16[64,512]{1,0:T(8,128)(2,1)}) %reduce-scatter.20.cloned.1.call-update) | async-done | bytes 65552 | tf_op jit(solution)/shard_map/reduce_scatter | solution.py:78
  248.2 0.9 convert_multiply_fusion.6
  249.2 5.3 %multiply_add_fusion = f32[64,4,64,128]{3,2,1,0:T(8,128)S(1)} fusion(f32[64,4,64,128]{3,2,1,0:T(8,128)} %param.18, f32[64,4,128]{2,1,0:T(4,128)S(1)} %mul.290, f32[64,4,64]{2,1,0:T(4,128)S(1)} %copy.21, f32[4]{0:T(128)S(1)} %exponential_subtract_fusion), kind=kLoop, calls=%fused_computation | loop fusion | flops 6291456 | bytes 16973840 | tf_op jit(solution)/shard_map/add | solution.py:100
  254.5 7.3 %fusion.30 = f32[64,4,1,128]{3,2,1,0:T(1,128)S(1)} fusion(f32[64,4,64,1]{2,3,1,0:T(1,128)S(1)} %copy.22, f32[64,4,64,128]{3,2,1,0:T(8,128)S(1)} %multiply_add_fusion), kind=kOutput, calls=%fused_computation.64 | convolution fusion | flops 25165824 | bytes 8585216 | tf_op jit(solution)/shard_map/bhk,bhkv->bhv/dot_general | solution.py:103
  262.0 0.2 multiply_reduce_fusion
  262.3 0.2 subtract_multiply_fusion
  262.5 12.8 %reduce-scatter.14.cloned.1.call-done = bf16[64,512]{1,0:T(8,128)(2,1)} async-done(((bf16[256,512]{1,0:T(8,128)(2,1)}), bf16[64,512]{1,0:T(8,128)(2,1)}) %reduce-scatter.14.cloned.1.call-update) | async-done | bytes 65552 | tf_op jit(solution)/shard_map/reduce_scatter | solution.py:81
  275.3 1.0 fusion.21
  276.3 9.3 %all_gather.28 = bf16[256,512]{1,0:T(8,128)(2,1)S(1)} all-gather(bf16[64,512]{1,0:T(8,128)(2,1)S(1)} %fusion.21), channel_id=1, replica_groups=mesh['kv'=4,'tp'=8] {'kv'}, dimensions={0}, use_global_device_ids=true | all-gather | bytes 327680 | tf_op jit(solution)/shard_map/all_gather | solution.py:111
  285.6 1.7 convolution_convert_fusion.4
  287.2 1.0 copy.26
  288.3 31.4 %reduce-scatter.24.cloned.1.call-done = bf16[128,256]{1,0:T(8,128)(2,1)} async-done(((bf16[1024,256]{1,0:T(8,128)(2,1)}), bf16[128,256]{1,0:T(8,128)(2,1)}) %reduce-scatter.24.cloned.1.call-update) | async-done | bytes 65552
  319.7 0.9 copy.27
  320.7 14.0 %all_gather.29 = bf16[256,1024]{1,0:T(8,128)(2,1)S(1)} all-gather(bf16[256,128]{1,0:T(8,128)(2,1)S(1)} %add_convert_fusion.1), channel_id=1, replica_groups=mesh['kv'=4,'tp'=8] {'tp'}, dimensions={1}, use_global_device_ids=true | all-gather | bytes 589824 | tf_op jit(solution)/shard_map/all_gather | solution.py:170
  334.8 3.7 convolution_convert_fusion
  338.5 3.7 convolution_convert_fusion.1
  342.4 10.3 %psum.31 = bf16[256]{0:T(256)(128)(2,1)S(1)} all-reduce(bf16[256]{0:T(256)(128)(2,1)S(1)} %fusion.7), channel_id=1, replica_groups=mesh['kv'=4,'tp'=8] {'kv'}, use_global_device_ids=true, to_apply=%region_16.17 | all-reduce | flops 256 | bytes 1024 | tf_op jit(solution)/shard_map/psum | solution.py:46
  352.8 25.9 %all-gather.7.cloned.1.call-done = bf16[1024,1408]{1,0:T(8,128)(2,1)} async-done(((bf16[256,1408]{1,0:T(8,128)(2,1)}), bf16[1024,1408]{1,0:T(8,128)(2,1)}) %all-gather.7.cloned.1.call-update) | async-done | bytes 2883600 | tf_op jit(solution)/shard_map/all_gather | solution.py:43
  378.7 3.3 reduce_sum.75
  382.0 47.3 %all-reduce.6.cloned.1.call-done = bf16[256,1408]{1,0:T(8,128)(2,1)} async-done(((bf16[256,1408]{1,0:T(8,128)(2,1)}), bf16[256,1408]{1,0:T(8,128)(2,1)}) %all-reduce.6.cloned.1.call-update) | async-done | bytes 720912 | tf_op jit(solution)/shard_map/psum | solution.py:42
  429.3 3.4 fusion.1
  432.7 1.0 copy.28
  433.8 31.6 %reduce-scatter.26.cloned.1.call-done = bf16[128,256]{1,0:T(8,128)(2,1)} async-done(((bf16[1024,256]{1,0:T(8,128)(2,1)}), bf16[128,256]{1,0:T(8,128)(2,1)}) %reduce-scatter.26.cloned.1.call-update) | async-done | bytes 65552
  465.3 0.9 copy.29
  466.3 0.7 add_convert_fusion
  (57 shorter events, 2.0 us)
Async XLA Ops:
  7.2 15.9 %copy-start = (bf16[1024,1408]{1,0:T(8,128)(2,1)S(1)}, bf16[1024,1408]{1,0:T(8,128)(2,1)}, u32[]{:S(2)}) copy-start(bf16[1024,1408]{1,0:T(8,128)(2,1)} %param.21) | copy-start | bytes 8650756
  7.2 60.2 %all-gather.5.cloned.1.call-start = ((), (), s32[]{:S(2)}) async-start(), calls=%async_computation.13 | async-start | bytes 3604480 | tf_op jit(solution)/shard_map/all_gather | solution.py:43
  23.0 2.7 copy-start.4
  25.6 92.5 %all-reduce.4.cloned.1.call-start = ((), (), s32[]{:S(2)}) async-start(), calls=%async_computation.7 | async-start | bytes 1441792 | tf_op jit(solution)/shard_map/psum | solution.py:42
  29.4 124.8 %reduce-scatter.22.cloned.1.call-start = ((), (), s32[]{:S(2)}) async-start(), calls=%async_computation.15 | async-start | bytes 589824
  70.7 84.5 %copy-start.2 = (bf16[256,128]{1,0:T(8,128)(2,1)S(1)}, bf16[256,128]{1,0:T(8,128)(2,1)}, u32[]{:S(2)}) copy-start(bf16[256,128]{1,0:T(8,128)(2,1)} %param.17) | copy-start | bytes 196612
  70.7 98.5 %copy-start.5 = (f32[1024]{0:T(1024)S(1)}, f32[1024]{0:T(1024)}, u32[]{:S(2)}) copy-start(f32[1024]{0:T(1024)} %param.23) | copy-start | bytes 12292
  121.6 49.7 %copy-start.7 = (u32[32]{0:T(128)S(1)}, u32[32]{0:T(128)}, u32[]{:S(2)}) copy-start(u32[32]{0:T(128)} %constant.56) | copy-start | bytes 388
  122.7 71.3 %reduce-scatter.16.cloned.1.call-start = ((), (), s32[]{:S(2)}) async-start(), calls=%async_computation.9 | async-start | bytes 163840 | tf_op jit(solution)/shard_map/reduce_scatter | solution.py:72
  171.3 49.4 %reduce-scatter.18.cloned.1.call-start = ((), (), s32[]{:S(2)}) async-start(), calls=%async_computation.10 | async-start | bytes 163840 | tf_op jit(solution)/shard_map/reduce_scatter | solution.py:75
  174.6 73.6 %reduce-scatter.20.cloned.1.call-start = ((), (), s32[]{:S(2)}) async-start(), calls=%async_computation.11 | async-start | bytes 327680 | tf_op jit(solution)/shard_map/reduce_scatter | solution.py:78
  177.1 98.2 %reduce-scatter.14.cloned.1.call-start = ((), (), s32[]{:S(2)}) async-start(), calls=%async_computation.8 | async-start | bytes 327680 | tf_op jit(solution)/shard_map/reduce_scatter | solution.py:81
  189.5 130.2 %reduce-scatter.24.cloned.1.call-start = ((), (), s32[]{:S(2)}) async-start(), calls=%async_computation.16 | async-start | bytes 589824
  254.5 7.4 %copy-start.1 = (f32[64,4,64,128]{3,2,1,0:T(8,128)}, f32[64,4,64,128]{3,2,1,0:T(8,128)S(1)}, u32[]{:S(2)}) copy-start(f32[64,4,64,128]{3,2,1,0:T(8,128)S(1)} %multiply_add_fusion) | copy-start | bytes 25165828
  254.5 20.8 %copy-start.3 = (f32[512]{0:T(512)S(1)}, f32[512]{0:T(512)}, u32[]{:S(2)}) copy-start(f32[512]{0:T(512)} %param.28) | copy-start | bytes 6148
  261.8 72.9 %copy-start.6 = (f32[1024]{0:T(1024)S(1)}, f32[1024]{0:T(1024)}, u32[]{:S(2)}) copy-start(f32[1024]{0:T(1024)} %param.30) | copy-start | bytes 12292
  288.3 90.4 %all-gather.7.cloned.1.call-start = ((), (), s32[]{:S(2)}) async-start(), calls=%async_computation.14 | async-start | bytes 3604480 | tf_op jit(solution)/shard_map/all_gather | solution.py:43
  338.4 90.9 %all-reduce.6.cloned.1.call-start = ((), (), s32[]{:S(2)}) async-start(), calls=%async_computation.12 | async-start | bytes 1441792 | tf_op jit(solution)/shard_map/psum | solution.py:42
  342.2 123.1 %reduce-scatter.26.cloned.1.call-start = ((), (), s32[]{:S(2)}) async-start(), calls=%async_computation.17 | async-start | bytes 589824
Sparse Core Ops, SparseCore 0:
  25.8 41.5 all-gather.4
  70.4 47.6 all-reduce.3
  122.8 31.3 reduce-scatter.21
  171.4 22.4 reduce-scatter.15
  196.5 24.1 reduce-scatter.17
  223.9 24.2 reduce-scatter.19
  250.9 24.3 reduce-scatter.13
  288.4 31.3 reduce-scatter.23
  338.6 40.0 all-gather.6
  381.6 47.6 all-reduce.5
  433.9 31.3 reduce-scatter.25
